TPU v7x, 32 devices: a whole 2x2x4 slice. The times are simulated.
32 devices in a mesh: grp: 2 (over y), kv: 4 (over z), tp: 4 (over x, core).
Axes of the slice: x: 2, y: 2, z: 4, core: 2. Of those that a mesh axis runs over, the one named last changes fastest.
Arguments:
- tokens: bfloat16 [16, 4096], P('grp', 'kv'), parts along dimension 0, may hold values from -6 to 6
- norm_gain: float32 [4096], replicated, may hold values from 0.1 to 1.9
- w_query: bfloat16 [4096, 4096], P('kv', 'tp'), may hold values from -0.09375 to 0.09375
- key_weight: bfloat16 [4096, 512], P('kv', 'tp'), may hold values from -0.09375 to 0.09375
- value_weight: bfloat16 [4096, 512], P('kv', 'tp'), may hold values from -0.09375 to 0.09375
- w_gate: bfloat16 [4096, 64], replicated, may hold values from -0.09375 to 0.09375
- gate_bias: float32 [64], replicated, may hold values from -3 to 4
- w_out: bfloat16 [4096, 4096], P('kv', 'tp'), may hold values from -0.1875 to 0.1875
- cache_keys: bfloat16 [16, 3072, 512], P('grp', 'kv', 'tp'), parts along dimension 0, may hold values from -240 to 240
- cache_values: bfloat16 [16, 3072, 512], P('grp', 'kv', 'tp'), parts along dimension 0, may hold values from -8 to 8
- cache_gate: float32 [16, 64, 3072], P('grp', 'tp', 'kv'), parts along dimension 0, may hold values from -3072 to 0, as said below
- gate_total: float32 [16, 64], P('grp', 'tp'), parts along dimension 0, may hold values from -3072 to 0, as said below
- lengths: int32 [16], P('grp'), parts along dimension 0, may hold values from 1536 to 3072, as said below
Outputs:
- mixed: bfloat16 [16, 4096], P('grp', 'kv'), parts along dimension 0
- key_new: bfloat16 [16, 512], P('grp', 'tp'), parts along dimension 0
- value_new: bfloat16 [16, 512], P('grp', 'tp'), parts along dimension 0
There are 2 independent parts, one for each index of `grp`. A program takes and returns all parts, laid end to end along the dimension named above; an argument that names none is the same for every part. Nothing has to cross between parts.
Inputs may be any that keep to these rules, and one draw needn't show every extreme that they name: `lengths`: one sequence of each draw has all 3072 positions cached. `cache_gate`: non-increasing along positions. `gate_total`: equal to cache_gate at position lengths - 1 of the same sequence and head.
All inputs are finite; a program needn't handle non-finite values.
Results may differ from a plain program's by a relative error of at most 0.015.
Values may be sent and summed in bfloat16 or wider, within the bound.
A program may use at most 64 MiB of HBM per device.

v0:
```python
import jax
import jax.numpy as jnp
from jax import lax
from jax.sharding import PartitionSpec as P

HEAD_SIZE = 64
NEG_FILL = -1e30


def per_device(
    tokens,
    norm_gain,
    w_query,
    key_weight,
    value_weight,
    w_gate,
    gate_bias,
    w_out,
    cache_keys,
    cache_values,
    cache_gate,
    gate_total,
    lengths,
):
    seq_count = tokens.shape[0]
    width_dev = tokens.shape[1]
    heads_dev = cache_gate.shape[1]
    positions_dev = cache_gate.shape[2]
    kv_heads_dev = cache_keys.shape[2] // HEAD_SIZE
    head_group = heads_dev // kv_heads_dev
    logit_scale = HEAD_SIZE ** (-0.5)
    whole = lax.all_gather(tokens, "kv", axis=1, tiled=True)
    features = whole.astype(jnp.float32)
    normed = (
        features
        * lax.rsqrt(jnp.mean(features * features, axis=-1, keepdims=True) + 1e-06)
        * norm_gain
    )
    normed = normed.astype(jnp.bfloat16)
    kv_index = lax.axis_index("kv")
    tp_index = lax.axis_index("tp")
    own_rows = lax.dynamic_slice_in_dim(normed, kv_index * width_dev, width_dev, 1)
    query_part = jnp.dot(own_rows, w_query, preferred_element_type=jnp.float32)
    key_part = jnp.dot(own_rows, key_weight, preferred_element_type=jnp.float32)
    value_part = jnp.dot(own_rows, value_weight, preferred_element_type=jnp.float32)
    query_sum, key_sum, value_sum = lax.psum((query_part, key_part, value_part), "kv")
    query = query_sum.astype(jnp.bfloat16)
    key_new = key_sum.astype(jnp.bfloat16)
    value_new = value_sum.astype(jnp.bfloat16)
    gate_cols = lax.dynamic_slice_in_dim(w_gate, tp_index * heads_dev, heads_dev, 1)
    bias_cols = lax.dynamic_slice_in_dim(gate_bias, tp_index * heads_dev, heads_dev, 0)
    log_gate = jax.nn.log_sigmoid(
        jnp.dot(normed, gate_cols, preferred_element_type=jnp.float32) + bias_cols
    )
    level = gate_total + log_gate
    query_head_rows = query.reshape(seq_count, kv_heads_dev, head_group, HEAD_SIZE)
    key_block = cache_keys.reshape(seq_count, positions_dev, kv_heads_dev, HEAD_SIZE)
    value_block = cache_values.reshape(seq_count, positions_dev, kv_heads_dev, HEAD_SIZE)
    score_matrix = (
        jnp.einsum(
            "skgd,spkd->skgp", query_head_rows, key_block, preferred_element_type=jnp.float32
        )
        * logit_scale
    )
    forget_bias = (level[:, :, None] - cache_gate).reshape(
        seq_count, kv_heads_dev, head_group, positions_dev
    )
    positions = kv_index * positions_dev + jnp.arange(positions_dev, dtype=jnp.int32)
    valid_mask = (positions[None, :] < lengths[:, None])[:, None, None, :]
    score_matrix = jnp.where(valid_mask, score_matrix + forget_bias, NEG_FILL)
    local_max = jnp.max(score_matrix, axis=-1)
    weights = jnp.where(valid_mask, jnp.exp(score_matrix - local_max[..., None]), 0.0)
    local_total = jnp.sum(weights, axis=-1)
    local_values = jnp.einsum(
        "skgp,spkd->skgd",
        weights.astype(jnp.bfloat16),
        value_block,
        preferred_element_type=jnp.float32,
    )
    block_max = lax.pmax(local_max, "kv")
    rescale = jnp.exp(local_max - block_max)
    block_total, block_values = lax.psum(
        (local_total * rescale, local_values * rescale[..., None]), "kv"
    )
    key_current = key_new.reshape(seq_count, kv_heads_dev, HEAD_SIZE)
    current_score = (
        jnp.einsum(
            "skgd,skd->skg", query_head_rows, key_current, preferred_element_type=jnp.float32
        )
        * logit_scale
    )
    top = jnp.maximum(block_max, current_score)
    cached_scale = jnp.exp(block_max - top)
    current_weight = jnp.exp(current_score - top)
    denominator = block_total * cached_scale + current_weight
    value_current = value_new.reshape(seq_count, kv_heads_dev, 1, HEAD_SIZE).astype(jnp.float32)
    total_sum = block_values * cached_scale[..., None] + current_weight[..., None] * value_current
    attended = (
        (total_sum / denominator[..., None])
        .reshape(seq_count, heads_dev * HEAD_SIZE)
        .astype(jnp.bfloat16)
    )
    partial_value = lax.dot_general(
        attended, w_out, (((1,), (1,)), ((), ())), preferred_element_type=jnp.float32
    )
    partial_value = lax.optimization_barrier(partial_value.astype(jnp.bfloat16)).astype(jnp.float32)
    mixed = lax.psum(partial_value.astype(jnp.bfloat16), "tp")
    return (mixed, key_new, value_new)


def solution(mesh):
    placed = (
        P("grp", "kv"),
        P(),
        P("kv", "tp"),
        P("kv", "tp"),
        P("kv", "tp"),
        P(),
        P(),
        P("kv", "tp"),
        P("grp", "kv", "tp"),
        P("grp", "kv", "tp"),
        P("grp", "tp", "kv"),
        P("grp", "tp"),
        P("grp"),
    )
    return jax.shard_map(
        per_device,
        mesh=mesh,
        in_specs=placed,
        out_specs=(P("grp", "kv"), P("grp", "tp"), P("grp", "tp")),
        check_vma=False,
    )
```

profile of v0, /device:TPU:0, one launch (start us, length us, event | category | flops | bytes accessed | tf_op | source)
XLA Modules:
  0.0 91.3 jit_solution(11908319094124294041)
XLA Ops:
  0.6 0.0 copy-start
  0.7 0.9 dynamic_slice.11
  1.5 0.7 broadcast_compare_fusion
  2.3 15.1 %all_gather.3 = bf16[8,4096]{1,0:T(8,128)(2,1)S(1)} all-gather(bf16[8,1024]{1,0:T(8,128)(2,1)} %param.13), channel_id=1, replica_groups=mesh['grp'=2,'kv'=4,'tp'=4] {'kv'}, dimensions={1}, use_global_device_ids=true | all-gather | bytes 81920 | tf_op jit(solution)/shard_map/all_gather | solution.py:32
  17.4 0.1 fusion.9
  17.5 0.8 fusion.11
  18.4 1.1 %fusion.22 = f32[8,16]{1,0:T(8,128)S(1)} fusion(f32[8,16]{1,0:T(8,128)} %param.24, bf16[8,4096]{1,0:T(8,128)(2,1)S(1)} %fusion.11, bf16[4096,64]{0,1:T(8,128)(2,1)} %param.18, s32[]{:T(128)S(6)} %select_n.20, f32[16]{0:T(128)S(1)} %dynamic_slice.11), kind=kOutput, calls=%fused_computation.35 | convolution fusion | flops 1049856 | bytes 201284 | tf_op jit(solution)/shard_map/dot_general | solution.py:53
  19.4 1.1 %fusion.15 = f32[8,128]{1,0:T(8,128)S(1)} fusion(bf16[1024,128]{1,0:T(8,128)(2,1)} %param.16, bf16[8,4096]{1,0:T(8,128)(2,1)S(1)} %fusion.11, s32[]{:T(128)S(6)} %select_n.19), kind=kOutput, calls=%fused_computation.24 | convolution fusion | flops 2097152 | bytes 282628 | tf_op jit(solution)/shard_map/dot_general | solution.py:44
  20.6 1.1 %fusion.13 = f32[8,128]{1,0:T(8,128)S(1)} fusion(bf16[1024,128]{1,0:T(8,128)(2,1)} %param.17, bf16[8,4096]{1,0:T(8,128)(2,1)S(1)} %fusion.11, s32[]{:T(128)S(6)} %select_n.19), kind=kOutput, calls=%fused_computation.22 | convolution fusion | flops 2097152 | bytes 282628 | tf_op jit(solution)/shard_map/dot_general | solution.py:45
  21.7 0.0 copy-done
  21.7 0.4 fusion.17
  22.0 19.1 %psum.42 = bf16[8,1024]{1,0:T(8,128)(2,1)S(1)} all-reduce(f32[8,1024]{1,0:T(8,128)S(1)} %fusion.17), channel_id=1, replica_groups=mesh['grp'=2,'kv'=4,'tp'=4] {'kv'}, use_global_device_ids=true, to_apply=%region_1.0 | all-reduce | flops 8192 | bytes 49152 | tf_op jit(solution)/shard_map/psum | solution.py:46
  41.2 0.1 reshape.76
  41.3 0.0 copy-start.1
  41.3 2.7 %copy.18 = bf16[8,768,128]{1,2,0:T(8,128)(2,1)} copy(bf16[8,768,128]{2,1,0:T(8,128)(2,1)} %param.21) | data formatting | bytes 3145728 | tf_op args[8]
  43.9 0.0 copy-done.1
  43.9 1.8 %fusion.33 = (f32[8,2,8]{2,1,0:T(2,128)S(1)}, f32[8,2,8,768]{3,2,1,0:T(8,128)S(1)}) fusion(f32[8,16,768]{2,1,0:T(8,128)S(1)} %copy-done.1, f32[8,16]{1,0:T(8,128)S(1)} %fusion.22, bf16[8,2,8,64]{3,2,1,0:T(8,128)(2,1)S(1)} %reshape.76, bf16[8,768,2,64]{1,3,2,0:T(8,128)(2,1)} %bitcast.24, pred[8,768]{1,0:T(8,128)(4,1)S(1)} %broadcast_compare_fusion), kind=kOutput, calls=%fused_computation.44 | convolution fusion | flops 13074304 | bytes 2382848 | tf_op jit(solution)/shard_map/skgd,spkd->skgp/dot_general | solution.py:60
  45.7 8.5 %pmax.7 = f32[8,2,8]{2,1,0:T(2,128)S(1)} all-reduce(f32[8,2,8]{2,1,0:T(2,128)S(1)} %get-tuple-element.12), channel_id=1, replica_groups=mesh['grp'=2,'kv'=4,'tp'=4] {'kv'}, use_global_device_ids=true, to_apply=%region_3.0 | all-reduce | flops 128 | bytes 1024 | tf_op jit(solution)/shard_map/pmax | solution.py:80
  54.3 0.2 fusion.3
  54.5 2.6 %copy.19 = bf16[8,768,128]{1,2,0:T(8,128)(2,1)} copy(bf16[8,768,128]{2,1,0:T(8,128)(2,1)} %param.22) | data formatting | bytes 3145728 | tf_op args[9]
  57.1 2.0 %convolution_multiply_fusion.1 = f32[8,2,8,64]{3,2,1,0:T(8,128)S(1)} fusion(bf16[8,768,2,64]{1,3,2,0:T(8,128)(2,1)} %bitcast.25, f32[8,2,8,768]{3,2,1,0:T(8,128)S(1)} %get-tuple-element.13, f32[8,2,8]{2,1,0:T(2,128)S(1)} %get-tuple-element.12, pred[8,768]{1,0:T(8,128)(4,1)S(1)} %broadcast_compare_fusion, f32[8,2,8]{2,1,0:T(2,128)S(1)} %bitcast.30), kind=kOutput, calls=%fused_computation.3 | convolution fusion | flops 12886016 | bytes 2006016 | tf_op jit(solution)/shard_map/skgp,spkd->skgd/dot_general | solution.py:74
  59.1 18.7 %all-reduce = (f32[8,2,8,64]{3,2,1,0:T(8,128)S(1)}, bf16[8,128]{1,0:T(8,128)(2,1)S(1)}, f32[8,2,8]{2,1,0:T(2,128)S(1)}, bf16[8,128]{1,0:T(8,128)(2,1)S(1)}) all-reduce(f32[8,2,8,64]{3,2,1,0:T(8,128)S(1)} %convolution_multiply_fusion.1, f32[8,128]{1,0:T(8,128)S(1)} %fusion.15, ...), channel_id=1, replica_groups=mesh['grp'=2,'kv'=4,'tp'=4] {'kv'}, use_global_device_ids=true, to_apply=%region_4.5 | all-reduce | flops 10368 | bytes 78848 | tf_op jit(solution)/shard_map/psum | solution.py:82
  77.8 0.0 copy-start.2
  77.8 0.0 copy-start.3
  77.8 0.1 reshape.85
  77.9 0.1 fusion.34
  78.1 0.1 reshape.81
  78.1 0.1 divide_convert_fusion
  78.3 0.1 convert_element_type.49
  78.4 2.2 %convolution_convert_fusion = bf16[8,1024]{1,0:T(8,128)(2,1)S(1)} fusion(bf16[8,1024]{1,0:T(8,128)(2,1)S(1)} %convert_element_type.49, bf16[1024,1024]{1,0:T(8,128)(2,1)} %param.20), kind=kOutput, calls=%fused_computation.4 | convolution fusion | flops 16785408 | bytes 2129920 | tf_op jit(solution)/shard_map/dot_general | solution.py:103
  80.6 10.7 %psum.47 = bf16[8,1024]{1,0:T(8,128)(2,1)} all-reduce(bf16[8,1024]{1,0:T(8,128)(2,1)S(1)} %convolution_convert_fusion), channel_id=1, replica_groups=mesh['grp'=2,'kv'=4,'tp'=4] {'tp'}, use_global_device_ids=true, to_apply=%region_9.10 | all-reduce | flops 8192 | bytes 32768 | tf_op jit(solution)/shard_map/psum | solution.py:107
  91.3 0.0 copy-done.2
  91.3 0.0 copy-done.3
  (4 shorter events, 0.1 us)
Async XLA Ops:
  0.6 21.0 %copy-start = (bf16[1024,1024]{1,0:T(8,128)(2,1)S(1)}, bf16[1024,1024]{1,0:T(8,128)(2,1)}, u32[]{:S(2)}) copy-start(bf16[1024,1024]{1,0:T(8,128)(2,1)} %param.15) | copy-start | bytes 6291460
  41.3 2.7 %copy-start.1 = (f32[8,16,768]{2,1,0:T(8,128)S(1)}, f32[8,16,768]{2,1,0:T(8,128)}, u32[]{:S(2)}) copy-start(f32[8,16,768]{2,1,0:T(8,128)} %param.23) | copy-start | bytes 1179652
  77.8 13.5 %copy-start.2 = (bf16[8,128]{1,0:T(8,128)(2,1)}, bf16[8,128]{1,0:T(8,128)(2,1)S(1)}, u32[]{:S(2)}) copy-start(bf16[8,128]{1,0:T(8,128)(2,1)S(1)} %get-tuple-element.4) | copy-start | bytes 6148
  77.8 13.5 %copy-start.3 = (bf16[8,128]{1,0:T(8,128)(2,1)}, bf16[8,128]{1,0:T(8,128)(2,1)S(1)}, u32[]{:S(2)}) copy-start(bf16[8,128]{1,0:T(8,128)(2,1)S(1)} %get-tuple-element.6) | copy-start | bytes 6148
where the time goes:
time: 91.8 us; the launch traced here: 91.3 us
  blocking collectives  72.2 us (79%)
  matrix products  9.82 us (11%)
  local copies, waits for them, and re-layouts  6.53 us (7%)
  other arithmetic  2.09 us (2%)
    psum x1, blocking collectives, per_device(): lax.psum((query_part, key_part, value_part), 'kv')  19.1 us
    psum x1, blocking collectives, per_device(): lax.psum((local_total * rescale, local_values * rescale[..., None]), 'kv')  18.7 us
    all_gather x1, blocking collectives, per_device(): whole = lax.all_gather(tokens, 'kv', axis=1, tiled=True)  15.1 us
    psum x1, blocking collectives, per_device(): mixed = lax.psum(partial_value.astype(jnp.bfloat16), 'tp')  10.7 us
    pmax x1, blocking collectives, per_device(): block_max = lax.pmax(local_max, 'kv')  8.5 us
    unnamed x10, local copies, waits for them, and re-layouts  5.29 us
    dot_general x1, matrix products, per_device(): lax.dot_general(attended, w_out, (((1,), (1,)), ((), ())), preferred_elem...  2.23 us
    dot_general x1, matrix products, per_device(): jnp.einsum('skgp,spkd->skgd', weights.astype(jnp.bfloat16), value_block,...  1.98 us

commit v1 on v0

--- a/solution.py
+++ b/solution.py
@@ -29,7 +29,12 @@
     kv_heads_dev = cache_keys.shape[2] // HEAD_SIZE
     head_group = heads_dev // kv_heads_dev
     logit_scale = HEAD_SIZE ** (-0.5)
-    whole = lax.all_gather(tokens, "kv", axis=1, tiled=True)
+    ring = [tokens]
+    for hop in range(3):
+        ring.append(lax.ppermute(ring[-1], "kv", [(dev, (dev + 1) % 4) for dev in range(4)]))
+    whole = jnp.roll(
+        jnp.concatenate(ring[::-1], axis=1), (lax.axis_index("kv") + 1) * ring[0].shape[1], axis=1
+    )
     features = whole.astype(jnp.float32)
     normed = (
         features

time: 91.8 us -> 86.3 us (0.940)
  blocking collectives: 72.2 us -> 57.4 us
  waiting for transfers between devices: 0 us -> 9.49 us
  starting transfers between devices: 0 us -> 3.11 us
  matrix products: 9.82 us -> 7.91 us
    all_gather x1 -> x0, blocking collectives: 15.1 us -> none  [per_device(): whole = lax.all_gather(tokens, 'kv', axis=1, tiled=True)]
    ppermute x0 -> x3, waiting for transfers between devices: none -> 9.49 us  [per_device(): lax.ppermute(ring[-1], 'kv', [(dev, (dev + 1) % 4) for dev in range(4)])]
    ppermute x0 -> x3, starting transfers between devices: none -> 3.11 us  [per_device(): lax.ppermute(ring[-1], 'kv', [(dev, (dev + 1) % 4) for dev in range(4)])]
    dot_general x1, matrix products: 1.11 us -> 0.15 us  [per_device(): key_part = jnp.dot(own_rows, key_weight, preferred_element_type=jnp.float32)]
    dot_general x1, matrix products: 1.1 us -> 0.15 us  [per_device(): jnp.dot(own_rows, value_weight, preferred_element_type=jnp.float32)]
    unnamed x10 -> x29, local copies, waits for them, and re-layouts: 5.29 us -> 5.34 us
  transfers between devices with their start and end apart: 0 -> 3, of which waited for: 0 -> 2; matrix products, arithmetic and copies ran while one was open for 0% -> 7% of each run, Pallas kernels for 0% -> 0%
where the time goes in v1:
time: 86.3 us; the launch traced here: 85.9 us
  blocking collectives  57.4 us (67%)
  waiting for transfers between devices  9.49 us (11%)
  matrix products  7.91 us (9%)
  local copies, waits for them, and re-layouts  5.77 us (7%)
  starting transfers between devices  3.11 us (4%)
  other arithmetic  1.38 us (2%)
    psum x1, blocking collectives, per_device(): lax.psum((query_part, key_part, value_part), 'kv')  19.5 us
    psum x1, blocking collectives, per_device(): lax.psum((local_total * rescale, local_values * rescale[..., None]), 'kv')  18.7 us
    psum x1, blocking collectives, per_device(): mixed = lax.psum(partial_value.astype(jnp.bfloat16), 'tp')  10.7 us
    ppermute x3, waiting for transfers between devices, per_device(): lax.ppermute(ring[-1], 'kv', [(dev, (dev + 1) % 4) for dev in range(4)])  9.49 us
    pmax x1, blocking collectives, per_device(): block_max = lax.pmax(local_max, 'kv')  8.5 us
    unnamed x29, local copies, waits for them, and re-layouts  5.34 us
    ppermute x3, starting transfers between devices, per_device(): lax.ppermute(ring[-1], 'kv', [(dev, (dev + 1) % 4) for dev in range(4)])  3.11 us
    dot_general x1, matrix products, per_device(): lax.dot_general(attended, w_out, (((1,), (1,)), ((), ())), preferred_elem...  2.23 us
  transfers between devices with their start and end apart: 3, of which 2 were waited for; matrix products, arithmetic and copies ran while one was open for 7% of the time, Pallas kernels for 0%

profile of v1, /device:TPU:0, one launch (start us, length us, event | category | flops | bytes accessed | tf_op | source)
XLA Modules:
  0.0 85.9 jit_solution(7290227401450269527)
XLA Ops:
  0.6 0.0 copy-start
  0.6 3.1 %collective-permute-start = (bf16[8,1024]{1,0:T(8,128)(2,1)}, bf16[8,1024]{1,0:T(8,128)(2,1)S(1)}, u32[]{:S(2)}, u32[]{:S(2)}) collective-permute-start(bf16[8,1024]{1,0:T(8,128)(2,1)} %param.13), channel_id=1, source_target_pairs={{0,4},{4,8},{8,12},{12,0},{1,5},{5,9},{9,13},{13,1},{2,6},{6,10},{... | collective-permute-start | bytes 49160 | tf_op jit(solution)/shard_map/ppermute | solution.py:34
  3.8 4.0 %collective-permute-done = bf16[8,1024]{1,0:T(8,128)(2,1)S(1)} collective-permute-done((bf16[8,1024]{1,0:T(8,128)(2,1)}, bf16[8,1024]{1,0:T(8,128)(2,1)S(1)}, u32[]{:S(2)}, u32[]{:S(2)}) %collective-permute-start) | collective-permute-done | bytes 16416 | tf_op jit(solution)/shard_map/ppermute | solution.py:34
  7.7 0.0 collective-permute-start.1
  7.7 5.5 %collective-permute-done.1 = bf16[8,1024]{1,0:T(8,128)(2,1)S(1)} collective-permute-done((bf16[8,1024]{1,0:T(8,128)(2,1)S(1)}, bf16[8,1024]{1,0:T(8,128)(2,1)S(1)}, u32[]{:S(2)}, u32[]{:S(2)}) %collective-permute-start.1) | collective-permute-done | bytes 16416 | tf_op jit(solution)/shard_map/ppermute | solution.py:34
  13.2 0.0 collective-permute-start.2
  13.2 0.7 broadcast_compare_fusion
  14.0 2.6 %copy.18 = bf16[8,768,128]{1,2,0:T(8,128)(2,1)} copy(bf16[8,768,128]{2,1,0:T(8,128)(2,1)} %param.21) | data formatting | bytes 3145728 | tf_op args[8]
  16.6 0.0 copy-start.9
  16.6 0.0 copy-start.4
  16.6 0.0 copy-start.5
  16.6 0.0 copy-start.2
  16.6 0.0 copy-start.3
  16.6 2.7 %copy.19 = bf16[8,768,128]{1,2,0:T(8,128)(2,1)} copy(bf16[8,768,128]{2,1,0:T(8,128)(2,1)} %param.22) | data formatting | bytes 3145728 | tf_op args[9]
  19.3 0.0 copy-done.9
  19.3 0.1 dynamic_slice.16
  19.3 0.0 collective-permute-done.2
  19.4 0.0 copy-done.4
  19.4 0.0 copy-start.6
  19.4 0.2 fusion.9
  19.6 0.0 copy-done.5
  19.6 0.0 copy-start.1
  19.6 0.1 fusion.11
  19.7 0.0 copy-done.2
  19.7 0.2 fusion.15
  19.9 0.0 copy-done.3
  19.9 0.1 fusion.13
  20.0 0.0 copy-done
  20.0 0.4 fusion.17
  20.4 19.5 %psum.42 = bf16[8,1024]{1,0:T(8,128)(2,1)S(1)} all-reduce(f32[8,1024]{1,0:T(8,128)S(1)} %fusion.17), channel_id=1, replica_groups=mesh['grp'=2,'kv'=4,'tp'=4] {'kv'}, use_global_device_ids=true, to_apply=%region_1.2 | all-reduce | flops 8192 | bytes 49152 | tf_op jit(solution)/shard_map/psum | solution.py:51
  39.9 0.1 reshape.76
  40.0 0.0 copy-done.6
  40.0 1.1 %fusion.22 = f32[8,16]{1,0:T(8,128)S(1)} fusion(f32[8,16]{1,0:T(8,128)S(1)} %copy-done.6, bf16[8,4096]{1,0:T(8,128)(2,1)S(1)} %fusion.11, bf16[4096,64]{0,1:T(8,128)(2,1)} %param.18, s32[]{:T(128)S(6)} %select_n.35, f32[16]{0:T(128)S(1)} %dynamic_slice.16), kind=kOutput, calls=%fused_computation.43 | convolution fusion | flops 1049856 | bytes 197700 | tf_op jit(solution)/shard_map/dot_general | solution.py:58
  41.1 0.0 copy-done.1
  41.1 1.8 %fusion.33 = (f32[8,2,8]{2,1,0:T(2,128)S(1)}, f32[8,2,8,768]{3,2,1,0:T(8,128)S(1)}) fusion(f32[8,16,768]{2,1,0:T(8,128)S(1)} %copy-done.1, f32[8,16]{1,0:T(8,128)S(1)} %fusion.22, bf16[8,2,8,64]{3,2,1,0:T(8,128)(2,1)S(1)} %reshape.76, bf16[8,768,2,64]{1,3,2,0:T(8,128)(2,1)} %bitcast.24, pred[8,768]{1,0:T(8,128)(4,1)S(1)} %broadcast_compare_fusion), kind=kOutput, calls=%fused_computation.52 | convolution fusion | flops 13074304 | bytes 2382848 | tf_op jit(solution)/shard_map/skgd,spkd->skgp/dot_general | solution.py:65
  42.9 8.5 %pmax.7 = f32[8,2,8]{2,1,0:T(2,128)S(1)} all-reduce(f32[8,2,8]{2,1,0:T(2,128)S(1)} %get-tuple-element.12), channel_id=1, replica_groups=mesh['grp'=2,'kv'=4,'tp'=4] {'kv'}, use_global_device_ids=true, to_apply=%region_3.4 | all-reduce | flops 128 | bytes 1024 | tf_op jit(solution)/shard_map/pmax | solution.py:85
  51.4 0.2 fusion.3
  51.7 2.0 %convolution_multiply_fusion.1 = f32[8,2,8,64]{3,2,1,0:T(8,128)S(1)} fusion(bf16[8,768,2,64]{1,3,2,0:T(8,128)(2,1)} %bitcast.25, f32[8,2,8,768]{3,2,1,0:T(8,128)S(1)} %get-tuple-element.13, f32[8,2,8]{2,1,0:T(2,128)S(1)} %get-tuple-element.12, pred[8,768]{1,0:T(8,128)(4,1)S(1)} %broadcast_compare_fusion, f32[8,2,8]{2,1,0:T(2,128)S(1)} %bitcast.30), kind=kOutput, calls=%fused_computation.3 | convolution fusion | flops 12886016 | bytes 2006016 | tf_op jit(solution)/shard_map/skgp,spkd->skgd/dot_general | solution.py:79
  53.7 18.7 %all-reduce = (f32[8,2,8,64]{3,2,1,0:T(8,128)S(1)}, bf16[8,128]{1,0:T(8,128)(2,1)S(1)}, f32[8,2,8]{2,1,0:T(2,128)S(1)}, bf16[8,128]{1,0:T(8,128)(2,1)S(1)}) all-reduce(f32[8,2,8,64]{3,2,1,0:T(8,128)S(1)} %convolution_multiply_fusion.1, f32[8,128]{1,0:T(8,128)S(1)} %fusion.15, ...), channel_id=1, replica_groups=mesh['grp'=2,'kv'=4,'tp'=4] {'kv'}, use_global_device_ids=true, to_apply=%region_4.5 | all-reduce | flops 10368 | bytes 78848 | tf_op jit(solution)/shard_map/psum | solution.py:87
  72.4 0.0 copy-start.7
  72.4 0.0 copy-start.8
  72.4 0.1 reshape.85
  72.5 0.1 fusion.34
  72.6 0.1 reshape.81
  72.7 0.1 divide_convert_fusion
  72.9 0.1 convert_element_type.49
  73.0 2.2 %convolution_convert_fusion = bf16[8,1024]{1,0:T(8,128)(2,1)S(1)} fusion(bf16[8,1024]{1,0:T(8,128)(2,1)S(1)} %convert_element_type.49, bf16[1024,1024]{1,0:T(8,128)(2,1)} %param.20), kind=kOutput, calls=%fused_computation.4 | convolution fusion | flops 16785408 | bytes 2129920 | tf_op jit(solution)/shard_map/dot_general | solution.py:108
  75.2 10.7 %psum.47 = bf16[8,1024]{1,0:T(8,128)(2,1)} all-reduce(bf16[8,1024]{1,0:T(8,128)(2,1)S(1)} %convolution_convert_fusion), channel_id=1, replica_groups=mesh['grp'=2,'kv'=4,'tp'=4] {'tp'}, use_global_device_ids=true, to_apply=%region_9.10 | all-reduce | flops 8192 | bytes 32768 | tf_op jit(solution)/shard_map/psum | solution.py:112
  85.9 0.0 copy-done.7
  85.9 0.0 copy-done.8
  (12 shorter events, 0.1 us)
Async XLA Ops:
  0.6 19.4 %copy-start = (bf16[1024,1024]{1,0:T(8,128)(2,1)S(1)}, bf16[1024,1024]{1,0:T(8,128)(2,1)}, u32[]{:S(2)}) copy-start(bf16[1024,1024]{1,0:T(8,128)(2,1)} %param.15) | copy-start | bytes 6291460
  0.6 7.1 %collective-permute-start = (bf16[8,1024]{1,0:T(8,128)(2,1)}, bf16[8,1024]{1,0:T(8,128)(2,1)S(1)}, u32[]{:S(2)}, u32[]{:S(2)}) collective-permute-start(bf16[8,1024]{1,0:T(8,128)(2,1)} %param.13), channel_id=1, source_target_pairs={{0,4},{4,8},{8,12},{12,0},{1,5},{5,9},{9,13},{13,1},{2,6},{6,10},{... | collective-permute-start | bytes 49160 | tf_op jit(solution)/shard_map/ppermute | solution.py:34
  7.7 5.5 %collective-permute-start.1 = (bf16[8,1024]{1,0:T(8,128)(2,1)S(1)}, bf16[8,1024]{1,0:T(8,128)(2,1)S(1)}, u32[]{:S(2)}, u32[]{:S(2)}) collective-permute-start(bf16[8,1024]{1,0:T(8,128)(2,1)S(1)} %collective-permute-done), channel_id=1, source_target_pairs={{0,4},{4,8},{8,12},{12,0},{1,5},{5,9},{9,13},{13,1},{2,6},{6,10},{... | collective-permute-start | bytes 49160 | tf_op jit(solution)/shard_map/ppermute | solution.py:34
  13.2 6.1 %collective-permute-start.2 = (bf16[8,1024]{1,0:T(8,128)(2,1)S(1)}, bf16[8,1024]{1,0:T(8,128)(2,1)S(1)}, u32[]{:S(2)}, u32[]{:S(2)}) collective-permute-start(bf16[8,1024]{1,0:T(8,128)(2,1)S(1)} %collective-permute-done.1), channel_id=1, source_target_pairs={{0,4},{4,8},{8,12},{12,0},{1,5},{5,9},{9,13},{13,1},{2,6},{6,10},{... | collective-permute-start | bytes 49160 | tf_op jit(solution)/shard_map/ppermute | solution.py:34
  16.6 2.7 %copy-start.9 = (f32[64]{0:T(128)S(1)}, f32[64]{0:T(128)}, u32[]{:S(2)}) copy-start(f32[64]{0:T(128)} %param.19) | copy-start | bytes 772
  16.6 2.8 %copy-start.4 = (bf16[8,1024]{1,0:T(8,128)(2,1)S(1)}, bf16[8,1024]{1,0:T(8,128)(2,1)}, u32[]{:S(2)}) copy-start(bf16[8,1024]{1,0:T(8,128)(2,1)} %param.13) | copy-start | bytes 49156
  16.6 3.0 %copy-start.5 = (f32[4096]{0:T(1024)S(1)}, f32[4096]{0:T(1024)}, u32[]{:S(2)}) copy-start(f32[4096]{0:T(1024)} %param.14) | copy-start | bytes 49156
  16.6 3.1 %copy-start.2 = (bf16[1024,128]{1,0:T(8,128)(2,1)S(1)}, bf16[1024,128]{1,0:T(8,128)(2,1)}, u32[]{:S(2)}) copy-start(bf16[1024,128]{1,0:T(8,128)(2,1)} %param.16) | copy-start | bytes 786436
  16.6 3.3 %copy-start.3 = (bf16[1024,128]{1,0:T(8,128)(2,1)S(1)}, bf16[1024,128]{1,0:T(8,128)(2,1)}, u32[]{:S(2)}) copy-start(bf16[1024,128]{1,0:T(8,128)(2,1)} %param.17) | copy-start | bytes 786436
  19.4 20.6 %copy-start.6 = (f32[8,16]{1,0:T(8,128)S(1)}, f32[8,16]{1,0:T(8,128)}, u32[]{:S(2)}) copy-start(f32[8,16]{1,0:T(8,128)} %param.24) | copy-start | bytes 1540
  19.6 21.5 %copy-start.1 = (f32[8,16,768]{2,1,0:T(8,128)S(1)}, f32[8,16,768]{2,1,0:T(8,128)}, u32[]{:S(2)}) copy-start(f32[8,16,768]{2,1,0:T(8,128)} %param.23) | copy-start | bytes 1179652
  72.4 13.5 %copy-start.7 = (bf16[8,128]{1,0:T(8,128)(2,1)}, bf16[8,128]{1,0:T(8,128)(2,1)S(1)}, u32[]{:S(2)}) copy-start(bf16[8,128]{1,0:T(8,128)(2,1)S(1)} %get-tuple-element.4) | copy-start | bytes 6148
  72.4 13.5 %copy-start.8 = (bf16[8,128]{1,0:T(8,128)(2,1)}, bf16[8,128]{1,0:T(8,128)(2,1)S(1)}, u32[]{:S(2)}) copy-start(bf16[8,128]{1,0:T(8,128)(2,1)S(1)} %get-tuple-element.6) | copy-start | bytes 6148
